TPU v7x, 32 devices: a whole 2x2x4 slice. The times are simulated.
32 devices in a mesh: sp: 16 (over z, y, x), tp: 2 (over core).
Axes of the slice: x: 2, y: 2, z: 4, core: 2. Of those that a mesh axis runs over, the one named last changes fastest.
Arguments:
- prompt: bfloat16 [2, 3072, 4096], P(None, 'sp'), as said below
- w_key: bfloat16 [4096, 2048], P('sp', 'tp'), may hold values from -0.09375 to 0.09375
- w_value: bfloat16 [4096, 4096], P('sp', 'tp'), may hold values from -0.09375 to 0.09375
- w_igate: bfloat16 [4096, 8], replicated, may hold values from -0.09375 to 0.09375
- w_fgate: bfloat16 [4096, 8], replicated, may hold values from -0.09375 to 0.09375
- input_bias: float32 [8], replicated, may hold values from -1 to 120
- forget_bias: float32 [8], replicated, may hold values from 4 to 20
- new_query: bfloat16 [2, 8, 256], P(None, 'tp'), may hold values from -6 to 6
- new_key: bfloat16 [2, 8, 256], P(None, 'tp'), may hold values from -6 to 6
- new_value: bfloat16 [2, 8, 512], P(None, 'tp'), may hold values from -6 to 6
- new_gates: float32 [2, 2, 8], P(None, None, 'tp'), may hold values from 2 to 9
Outputs:
- cache_memory: bfloat16 [2, 8, 256, 512], P(None, 'tp', 'sp')
- cache_norm: float32 [2, 8, 256], P(None, 'tp', 'sp')
- cache_max: float32 [2, 8], P(None, 'tp')
- first_read: bfloat16 [2, 8, 512], P(None, 'tp')
Inputs may be any that keep to these rules, and one draw needn't show every extreme that they name: `prompt`: Real-valued features, each entry drawn independently; their magnitude differs from one block of 192 positions to the next.
All inputs are finite; a program needn't handle non-finite values.
Results may differ from a plain program's by a relative error of at most 0.019.
Values may be sent and summed in bfloat16 or wider, within the bound.
A program may use at most 64 MiB of HBM per device.

v0:
```python
import jax
import jax.numpy as jnp
from jax import lax
from jax.sharding import PartitionSpec as P


def entering(value, axis, join, neutral):
    count, mine = (lax.axis_size(axis), lax.axis_index(axis))
    pieces = lax.all_gather(value, axis)
    pieces = pieces[::-1]
    mine = count - 1 - mine
    so_far = jnp.full_like(value, 0) + jnp.asarray(neutral, value.dtype)

    def turn(position, so_far):
        longer = join(so_far, pieces[position])
        return jnp.where(position < mine, longer, so_far)

    return lax.fori_loop(0, count - 1, turn, so_far)


def add_pair(earlier, later):
    return earlier + later


def per_device(
    prompt,
    w_key,
    w_value,
    w_igate,
    w_fgate,
    input_bias,
    forget_bias,
    new_query,
    new_key,
    new_value,
    new_gates,
):
    seq_count, span_len, model_width = prompt.shape
    local_heads = new_query.shape[1]
    key_size = new_query.shape[2]
    value_size = new_value.shape[2]
    key_scale = key_size ** (-0.5)
    token_rows = prompt.reshape(seq_count * span_len, model_width)
    whole_key, whole_value = (
        lax.all_gather(w_key, "sp", axis=0, tiled=True),
        lax.all_gather(w_value, "sp", axis=0, tiled=True),
    )
    key_rows = jnp.dot(token_rows, whole_key, preferred_element_type=jnp.float32).astype(
        jnp.bfloat16
    )
    value_rows = jnp.dot(token_rows, whole_value, preferred_element_type=jnp.float32).astype(
        jnp.bfloat16
    )
    head_start = lax.axis_index("tp") * local_heads
    input_all = jnp.dot(token_rows, w_igate, preferred_element_type=jnp.float32) + input_bias
    forget_all = jnp.dot(token_rows, w_fgate, preferred_element_type=jnp.float32) + forget_bias
    input_gate = lax.dynamic_slice_in_dim(input_all, head_start, local_heads, 1).reshape(
        seq_count, span_len, local_heads
    )
    log_forget = jax.nn.log_sigmoid(
        lax.dynamic_slice_in_dim(forget_all, head_start, local_heads, 1)
    ).reshape(seq_count, span_len, local_heads)
    block_total = jnp.sum(log_forget, axis=1)
    forget_after = block_total[:, None] - jnp.cumsum(log_forget, axis=1)
    log_weight = forget_after + input_gate
    block_max = jnp.max(log_weight, axis=1)
    key_blocks = key_rows.reshape(seq_count, span_len, local_heads, key_size).astype(jnp.float32)
    decayed = (jnp.exp(log_weight - block_max[:, None])[..., None] * key_scale * key_blocks).astype(
        jnp.bfloat16
    )
    value_blocks = value_rows.reshape(seq_count, span_len, local_heads, value_size)
    block_norm = jnp.sum(decayed.astype(jnp.float32), axis=1)
    later_total = entering(block_total, "sp", add_pair, jnp.zeros_like(block_total))
    block_lift = later_total + block_max
    global_max = lax.pmax(block_lift, "sp")
    factor = jnp.exp(block_lift - global_max)
    scaled_norm = factor[:, :, None] * block_norm
    query_full = new_query.astype(jnp.float32)
    block_state = jnp.einsum(
        "sthk,sthv->shkv", decayed, value_blocks, preferred_element_type=jnp.float32
    )
    scaled_state = factor[:, :, None, None] * block_state
    memory_rows, norm_rows = (
        lax.psum_scatter(scaled_state, "sp", scatter_dimension=2, tiled=True),
        lax.psum_scatter(scaled_norm, "sp", scatter_dimension=2, tiled=True),
    )
    token_score = jnp.einsum(
        "shk,sthk->sth", new_query, decayed, preferred_element_type=jnp.float32
    )
    score_high = token_score.astype(jnp.bfloat16)
    score_low = (token_score - score_high.astype(jnp.float32)).astype(jnp.bfloat16)
    weighted = jnp.einsum(
        "sth,sthv->shv", score_high, value_blocks, preferred_element_type=jnp.float32
    )
    weighted = weighted + jnp.einsum(
        "sth,sthv->shv", score_low, value_blocks, preferred_element_type=jnp.float32
    )
    partial_state = factor[..., None] * weighted
    partial_norm = jnp.sum(query_full * scaled_norm, axis=-1)
    query_state, query_norm = lax.psum((partial_state, partial_norm), "sp")
    forget_new = jax.nn.log_sigmoid(new_gates[1])
    input_new = new_gates[0]
    mixed = jnp.maximum(forget_new + global_max, input_new)
    carried = jnp.exp(forget_new + global_max - mixed)
    fresh = jnp.exp(input_new - mixed)
    own_score = jnp.sum(query_full * new_key.astype(jnp.float32), axis=-1) * key_scale
    numer = carried[..., None] * query_state + (fresh * own_score)[..., None] * new_value.astype(
        jnp.float32
    )
    denom = carried * query_norm + fresh * own_score
    first_read = (numer / jnp.maximum(jnp.abs(denom), 1.0)[..., None]).astype(jnp.bfloat16)
    return (memory_rows.astype(jnp.bfloat16), norm_rows, global_max, first_read)


def solution(mesh):
    placed = (
        P(None, "sp", None),
        P("sp", "tp"),
        P("sp", "tp"),
        P(),
        P(),
        P(),
        P(),
        P(None, "tp", None),
        P(None, "tp", None),
        P(None, "tp", None),
        P(None, None, "tp"),
    )
    return jax.shard_map(
        per_device,
        mesh=mesh,
        in_specs=placed,
        out_specs=(
            P(None, "tp", "sp", None),
            P(None, "tp", "sp"),
            P(None, "tp"),
            P(None, "tp", None),
        ),
        check_vma=False,
    )
```

profile of v0, /device:TPU:0, one launch (start us, length us, event | category | flops | bytes accessed | tf_op | source)
XLA Modules:
  0.0 501.1 jit_solution(298279706807457134)
XLA Ops:
  7.2 0.7 all-gather.5.cloned.1.call-update
  8.0 0.7 all-gather.7.cloned.1.call-update
  8.7 0.7 dynamic-slice
  9.5 0.7 dynamic-slice.1
  10.2 1.7 fusion.30
  12.0 0.9 fusion.31
  13.3 2.4 reduce-window.6
  16.3 43.4 %all-gather.1 = f32[16,2,4]{2,1,0:T(2,128)S(1)} all-gather(f32[1,2,4]{2,1,0:T(2,128)S(1)} %bitcast.71), channel_id=2, replica_groups=mesh['sp'=16,'tp'=2] {'sp'}, dimensions={0}, use_global_device_ids=true | all-gather | bytes 544 | tf_op jit(solution)/shard_map/all_gather | solution.py:9
  59.7 0.6 while.14
  60.4 0.2 fusion.26
  60.5 38.3 %pmax.7 = f32[2,4]{0,1:T(4,128)S(1)} all-reduce(f32[2,4]{0,1:T(4,128)S(1)} %add.94), channel_id=1, replica_groups=mesh['sp'=16,'tp'=2] {'sp'}, use_global_device_ids=true, to_apply=%region_6.7 | all-reduce | flops 8 | bytes 64 | tf_op jit(solution)/shard_map/pmax | solution.py:75
  99.0 27.4 %all-gather.5.cloned.1.call-done = bf16[4096,1024]{1,0:T(8,128)(2,1)} async-done(((bf16[256,1024]{1,0:T(8,128)(2,1)}), bf16[4096,1024]{1,0:T(8,128)(2,1)}) %all-gather.5.cloned.1.call-update) | async-done | bytes 8388624 | tf_op jit(solution)/shard_map/all_gather | solution.py:45
  126.5 7.0 %fusion.1 = f32[384,1024]{1,0:T(8,128)} fusion(bf16[384,4096]{1,0:T(8,128)(2,1)S(1)} %bitcast.61, bf16[4096,1024]{1,0:T(8,128)(2,1)} %all-gather.5.cloned.1.call-done), kind=kOutput, calls=%fused_computation.7 | convolution fusion | flops 3222011904 | bytes 13107200 | tf_op jit(solution)/shard_map/dot_general | solution.py:48
  133.5 2.9 reshape.51
  136.4 2.8 convert_reduce_fusion
  139.3 0.2 copy.83
  139.5 0.8 reshape.63
  140.4 178.5 %all-gather.7.cloned.1.call-done = bf16[4096,2048]{1,0:T(8,128)(2,1)} async-done(((bf16[256,2048]{1,0:T(8,128)(2,1)}), bf16[4096,2048]{1,0:T(8,128)(2,1)}) %all-gather.7.cloned.1.call-update) | async-done | bytes 16777232 | tf_op jit(solution)/shard_map/all_gather | solution.py:46
  319.0 11.6 %convolution_convert_fusion = bf16[384,2048]{1,0:T(8,128)(2,1)} fusion(bf16[384,4096]{1,0:T(8,128)(2,1)S(1)} %bitcast.62, bf16[4096,2048]{1,0:T(8,128)(2,1)} %all-gather.7.cloned.1.call-done), kind=kOutput, calls=%fused_computation.1 | convolution fusion | flops 6443237376 | bytes 21495808 | tf_op jit(solution)/shard_map/dot_general | solution.py:51
  330.5 3.9 reshape.50
  334.4 4.6 convolution_multiply_fusion
  339.0 0.6 copy.76
  339.9 1.4 fusion.15
  341.5 55.5 %reduce-scatter.7.cloned.1.call-done = f32[16,8]{1,0:T(8,128)} async-done(((f32[256,8]{1,0:T(8,128)}), f32[16,8]{1,0:T(8,128)}) %reduce-scatter.7.cloned.1.call-update) | async-done | bytes 528
  397.0 0.8 reshape.64
  397.7 0.7 copy.84
  398.4 1.8 fusion.2
  400.2 1.9 fusion.4
  402.2 72.6 %all-reduce.1 = (f32[2,4,512]{2,1,0:T(4,128)S(1)}, f32[2,4]{0,1:T(4,128)S(1)}) all-reduce(f32[2,4,512]{2,1,0:T(4,128)S(1)} %fusion.7, f32[2,4]{0,1:T(4,128)S(1)} %copy.74), channel_id=1, replica_groups=mesh['sp'=16,'tp'=2] {'sp'}, use_global_device_ids=true, to_apply=%region_10.11 | all-reduce | flops 4104 | bytes 32832 | tf_op jit(solution)/shard_map/psum | solution.py:100
  475.1 0.7 fusion.8
  475.8 17.2 %reduce-scatter.5.cloned.1.call-done = f32[2,4,16,512]{3,2,1,0:T(8,128)} async-done(((f32[2,4,256,512]{3,2,1,0:T(8,128)}), f32[2,4,16,512]{3,2,1,0:T(8,128)}) %reduce-scatter.5.cloned.1.call-update) | async-done | bytes 262160 | tf_op jit(solution)/shard_map/reduce_scatter | solution.py:84
  492.9 1.6 convert_element_type.47
  (70 shorter events, 2.6 us)
Async XLA Ops:
  7.2 3.0 copy-start
  7.2 4.8 copy-start.1
  7.2 119.3 %all-gather.5.cloned.1.call-start = ((), (), s32[]{:S(2)}) async-start(), calls=%async_computation.2 | async-start | bytes 8912896 | tf_op jit(solution)/shard_map/all_gather | solution.py:45
  7.9 311.0 %all-gather.7.cloned.1.call-start = ((), (), s32[]{:S(2)}) async-start(), calls=%async_computation.3 | async-start | bytes 17825792 | tf_op jit(solution)/shard_map/all_gather | solution.py:46
  8.7 388.3 %reduce-scatter.7.cloned.1.call-start = ((), (), s32[]{:S(2)}) async-start(), calls=%async_computation.5 | async-start | bytes 139264
  133.5 5.7 %copy-start.2 = (bf16[2,4,256]{2,1,0:T(4,128)(2,1)S(1)}, bf16[2,4,256]{2,1,0:T(4,128)(2,1)}, u32[]{:S(2)}) copy-start(bf16[2,4,256]{2,1,0:T(4,128)(2,1)} %param.20) | copy-start | bytes 12292
  133.5 5.7 %copy-start.4 = (bf16[2,4,256]{2,1,0:T(4,128)(2,1)S(1)}, bf16[2,4,256]{2,1,0:T(4,128)(2,1)}, u32[]{:S(2)}) copy-start(bf16[2,4,256]{2,1,0:T(4,128)(2,1)} %param.21) | copy-start | bytes 12292
  140.4 352.6 %reduce-scatter.5.cloned.1.call-start = ((), (), s32[]{:S(2)}) async-start(), calls=%async_computation.4 | async-start | bytes 4456448 | tf_op jit(solution)/shard_map/reduce_scatter | solution.py:84
  339.0 0.7 copy-start.5
  339.0 136.1 %copy-start.3 = (bf16[2,4,512]{2,1,0:T(4,128)(2,1)S(1)}, bf16[2,4,512]{2,1,0:T(4,128)(2,1)}, u32[]{:S(2)}) copy-start(bf16[2,4,512]{2,1,0:T(4,128)(2,1)} %param.22) | copy-start | bytes 24580
Sparse Core Ops, SparseCore 0:
  10.8 115.6 all-gather.4
  129.2 189.6 all-gather.6
  321.8 75.1 reduce-scatter.6
  399.1 93.7 reduce-scatter.4
where the time goes:
time: 502 us; the launch traced here: 501 us
  waiting for transfers between devices  280 us (56%)
  blocking collectives  154 us (31%)
  matrix products  31 us (6%)
  between operations  13.9 us (3%)
  local copies, waits for them, and re-layouts  12.9 us (3%)
  other arithmetic  8.55 us (2%)
    all_gather x1, waiting for transfers between devices, per_device(): lax.all_gather(w_value, 'sp', axis=0, tiled=True)  179 us
    psum x1, blocking collectives, per_device(): query_state, query_norm = lax.psum((partial_state, partial_norm), 'sp')  72.6 us
    unnamed x5, waiting for transfers between devices  56.9 us
    all_gather x1, blocking collectives, entering(): pieces = lax.all_gather(value, axis)  43.4 us
    pmax x1, blocking collectives, per_device(): global_max = lax.pmax(block_lift, 'sp')  38.3 us
    all_gather x1, waiting for transfers between devices, per_device(): lax.all_gather(w_key, 'sp', axis=0, tiled=True)  27.4 us
    reduce_scatter x1, waiting for transfers between devices, per_device(): lax.psum_scatter(scaled_state, 'sp', scatter_dimension=2, tiled=True)  17.2 us
    dot_general x1, matrix products, per_device(): jnp.dot(token_rows, whole_value, preferred_element_type=jnp.float32)  11.6 us
  transfers between devices with their start and end apart: 4, of which 4 were waited for; matrix products, arithmetic and copies ran while one was open for 10% of the time, Pallas kernels for 0%

commit v1 on v0

--- a/solution.py
+++ b/solution.py
@@ -1,7 +1,516 @@
+import functools
 import jax
 import jax.numpy as jnp
 from jax import lax
+from jax.experimental import pallas as pl
+from jax.experimental.pallas import tpu as pltpu
 from jax.sharding import PartitionSpec as P
+
+CHUNKS = 4
+HIGH = lax.Precision.HIGHEST
+
+
+def flip(bit, change):
+    return bit + change - 2 * bit * change
+
+
+def log_sigmoid(v):
+    return jnp.minimum(v, 0.0) - jnp.log1p(jnp.exp(-jnp.abs(v)))
+
+
+def kernel(
+    prompt,
+    w_key,
+    w_value,
+    w_gate,
+    gate_bias,
+    new_query,
+    new_key,
+    new_value,
+    new_gates,
+    memory_out,
+    norm_out,
+    max_out,
+    read_out,
+    xb,
+    wk,
+    wv,
+    decay,
+    vals,
+    weight,
+    stat,
+    state,
+    aux,
+    rmem,
+    raux,
+    local_sem,
+    x_send,
+    x_recv,
+    d_send,
+    d_recv,
+    wk_send,
+    wk_recv,
+    wv_send,
+    wv_recv,
+    s_send,
+    s_recv,
+    m_send,
+    m_recv,
+    a_send,
+    a_recv,
+):
+    count = lax.axis_size("sp")
+    me = lax.axis_index("sp")
+    core = lax.axis_index("tp")
+    seqs, span, width = prompt.shape
+    depth = w_key.shape[0]
+    heads = new_query.shape[1]
+    dk = new_query.shape[2]
+    dv = new_value.shape[2]
+    total_heads = gate_bias.shape[1] // 2
+    key_scale = dk ** (-0.5)
+    cut = width // CHUNKS
+    rows_out = dk // count
+    zh, zl, y, x = me // 8, (me // 4) % 2, (me // 2) % 2, me % 2
+    mine = zl * 2 + x
+
+    def place(dh, dy, dz, dx):
+        return flip(zh, dh) * 8 + flip(zl, dz) * 4 + flip(y, dy) * 2 + flip(x, dx)
+
+    def remote(src, dst, send, recv, sp, tp):
+        return pltpu.make_async_remote_copy(
+            src_ref=src,
+            dst_ref=dst,
+            send_sem=send,
+            recv_sem=recv,
+            device_id=(sp, tp),
+            device_id_type=pl.DeviceIdType.MESH,
+        )
+
+    ring = [(0, 0), (0, 1), (1, 0), (1, 1)]
+    clique = [(0, 0), (0, 1), (1, 0), (1, 1)]
+    sent = []
+
+    def go(copy):
+        copy.start()
+        sent.append(copy)
+
+    barrier = pltpu.get_barrier_semaphore()
+    for off in range(1, count):
+        pl.semaphore_signal(
+            barrier,
+            inc=1,
+            device_id=((me + off) % count, core),
+            device_id_type=pl.DeviceIdType.MESH,
+        )
+    pl.semaphore_signal(
+        barrier, inc=1, device_id=(me, 1 - core), device_id_type=pl.DeviceIdType.MESH
+    )
+
+    def w_rows(slot):
+        q, r = slot // 4, slot % 4
+        src = place(*clique[q], *ring[r])
+        return pl.ds(pl.multiple_of(src * depth, depth), depth)
+
+    own_x = []
+    for s in range(seqs):
+        c = pltpu.make_async_copy(
+            prompt.at[s], xb.at[0, pl.ds(s * span, span)], local_sem.at[s]
+        )
+        c.start()
+        own_x.append(c)
+    kcols = pl.ds(pl.multiple_of(mine * dk, dk), dk)
+    vcols = pl.ds(pl.multiple_of(mine * dv, dv), dv)
+    own_rows = w_rows(0)
+    own_k = pltpu.make_async_copy(w_key.at[:, kcols], wk.at[own_rows], local_sem.at[2])
+    own_v = pltpu.make_async_copy(w_value.at[:, vcols], wv.at[own_rows], local_sem.at[3])
+    own_k.start()
+    own_v.start()
+    pl.semaphore_wait(barrier, count)
+
+    for r in (1, 2, 3):
+        dz, dx = ring[r]
+        peer = place(0, 0, dz, dx)
+        theirs = flip(zl, dz) * 2 + flip(x, dx)
+        kc = pl.ds(pl.multiple_of(theirs * dk, dk), dk)
+        vc = pl.ds(pl.multiple_of(theirs * dv, dv), dv)
+        go(remote(w_key.at[:, kc], wk.at[own_rows], wk_send.at[r], wk_recv.at[r], peer, core))
+        go(remote(w_value.at[:, vc], wv.at[own_rows], wv_send.at[r], wv_recv.at[r], peer, core))
+
+    def w_relay(slot, to, tag):
+        rows = w_rows(slot)
+        q = slot // 4
+        there = (q + to[0] * 2 + to[1]) * 4 + slot % 4
+        peer = place(to[0], to[1], 0, 0)
+        go(remote(wk.at[rows], wk.at[rows], wk_send.at[tag], wk_recv.at[there], peer, core))
+        go(remote(wv.at[rows], wv.at[rows], wv_send.at[tag], wv_recv.at[there], peer, core))
+
+    def w_wait(slot):
+        rows = w_rows(slot)
+        pltpu.make_async_copy(wk.at[rows], wk.at[rows], wk_recv.at[slot]).wait()
+        pltpu.make_async_copy(wv.at[rows], wv.at[rows], wv_recv.at[slot]).wait()
+
+    def x_part(slot, seq_rows, k):
+        return xb.at[slot, seq_rows, pl.ds(k * cut, cut)]
+
+    my_rows = pl.ds(pl.multiple_of(core * span, span), span)
+    other_rows = pl.ds(pl.multiple_of((1 - core) * span, span), span)
+    to_x, to_z = place(0, 0, 0, 1), place(0, 0, 1, 0)
+
+    def x_send_own(slot, k, peer):
+        go(
+            remote(
+                prompt.at[core, :, pl.ds(k * cut, cut)],
+                x_part(slot, my_rows, k),
+                x_send.at[slot, k],
+                x_recv.at[slot, k],
+                peer,
+                core,
+            )
+        )
+
+    def x_wait(slot, k):
+        part = x_part(slot, my_rows, k)
+        pltpu.make_async_copy(part, part, x_recv.at[slot, k]).wait()
+
+    def x_across(slot, k):
+        part = x_part(slot, my_rows, k)
+        go(remote(part, part, d_send.at[slot, k], d_recv.at[slot, k], me, 1 - core))
+
+    def d_wait(slot, k):
+        part = x_part(slot, other_rows, k)
+        pltpu.make_async_copy(part, part, d_recv.at[slot, k]).wait()
+
+    x_send_own(2, 0, to_z)
+    for k in range(CHUNKS):
+        x_send_own(1, k, to_x)
+    own_k.wait()
+    own_v.wait()
+    w_relay(0, (1, 0), 4)
+    w_relay(0, (0, 1), 8)
+    for r in (1, 2, 3):
+        w_wait(r)
+        w_relay(r, (1, 0), 4 + r)
+        w_relay(r, (0, 1), 8 + r)
+        x_send_own(2, r, to_z)
+    for c in own_x:
+        c.wait()
+
+    lane = lax.broadcasted_iota(jnp.int32, (seqs * span, 2 * total_heads), 1)
+    head = core * heads + mine
+    at_t = lax.broadcasted_iota(jnp.int32, (span, span), 0)
+    at_u = lax.broadcasted_iota(jnp.int32, (span, span), 1)
+    after = (at_u > at_t).astype(jnp.float32)
+    stat_row = lax.broadcasted_iota(jnp.int32, (8, 128), 0)
+    stat_lane = lax.broadcasted_iota(jnp.int32, (8, 128), 1)
+
+    def gates(r, table):
+        both = jnp.dot(xb[r], w_gate[...], preferred_element_type=jnp.float32) + gate_bias[...]
+        gate_in = jnp.sum(jnp.where(lane == head, both, 0.0), axis=1, keepdims=True)
+        gate_f = jnp.sum(
+            jnp.where(lane == total_heads + head, both, 0.0), axis=1, keepdims=True
+        )
+        forget = log_sigmoid(gate_f)
+        for s in range(seqs):
+            part = forget[s * span : (s + 1) * span]
+            wide = jnp.broadcast_to(part, (span, 128))
+            later = jnp.dot(after, wide, precision=HIGH, preferred_element_type=jnp.float32)
+            level = later[:, 0:1] + gate_in[s * span : (s + 1) * span]
+            top = jnp.max(level, axis=0, keepdims=True)
+            total = jnp.sum(part, axis=0, keepdims=True)
+            weight[r, s * span : (s + 1) * span] = jnp.broadcast_to(
+                jnp.exp(level - top) * key_scale, (span, 128)
+            )
+            hit = stat_row == r * seqs + s
+            table = jnp.where(hit & (stat_lane == 0), total, table)
+            table = jnp.where(hit & (stat_lane == 1), top, table)
+        return table
+
+    table = gates(0, jnp.zeros((8, 128), jnp.float32))
+    for k in range(CHUNKS):
+        w_wait(8 + k)
+        w_relay(8 + k, (0, 1), 12 + k)
+        x_wait(2, k)
+        go(
+            remote(
+                x_part(2, my_rows, k),
+                x_part(3, my_rows, k),
+                x_send.at[3, k],
+                x_recv.at[3, k],
+                to_x,
+                core,
+            )
+        )
+        x_across(2, k)
+        x_wait(1, k)
+        x_across(1, k)
+    for k in range(CHUNKS):
+        d_wait(1, k)
+        d_wait(2, k)
+    table = gates(1, table)
+    table = gates(2, table)
+    for k in range(CHUNKS):
+        x_wait(3, k)
+        x_across(3, k)
+    for k in range(CHUNKS):
+        d_wait(3, k)
+    table = gates(3, table)
+    stat[0] = table
+    for slot in (4, 5, 6, 7, 12, 13, 14, 15):
+        w_wait(slot)
+
+    def project(r, carry):
+        def step(k, acc):
+            at = pl.ds(pl.multiple_of(k * cut, cut), cut)
+            rows = xb[r, :, at]
+            return (
+                acc[0] + jnp.dot(rows, wk[at], preferred_element_type=jnp.float32),
+                acc[1] + jnp.dot(rows, wv[at], preferred_element_type=jnp.float32),
+            )
+
+        keys, values = lax.fori_loop(
+            0,
+            CHUNKS,
+            step,
+            (
+                jnp.zeros((seqs * span, dk), jnp.float32),
+                jnp.zeros((seqs * span, dv), jnp.float32),
+            ),
+        )
+        keys = keys.astype(jnp.bfloat16).astype(jnp.float32)
+        decay[r] = (weight[r, :, 0:1] * keys).astype(jnp.bfloat16)
+        vals[r] = values.astype(jnp.bfloat16)
+        return carry
+
+    project(0, 0)
+    for q in (1, 2, 3):
+        dh, dy = clique[q]
+        go(
+            remote(
+                stat.at[0], stat.at[q], s_send.at[q], s_recv.at[q], place(dh, dy, 0, 0), core
+            )
+        )
+    lax.fori_loop(1, 4, project, 0)
+    for q in (1, 2, 3):
+        pltpu.make_async_copy(stat.at[q], stat.at[q], s_recv.at[q]).wait()
+
+    stats = jnp.concatenate([stat[q] for q in range(4)], axis=0)
+
+    def spot(dim):
+        n = lax.broadcasted_iota(jnp.int32, (32, 32), dim)
+        dh, dy, dz, dx = n // 16, (n // 8) % 2, (n // 4) % 2, (n // 2) % 2
+        where = flip(zh, dh) * 8 + flip(zl, dz) * 4 + flip(y, dy) * 2 + flip(x, dx)
+        return where, n % 2
+
+    (pos_a, seq_a), (pos_b, seq_b) = spot(0), spot(1)
+    later_mask = ((pos_b > pos_a) & (seq_a == seq_b)).astype(jnp.float32)
+    later = jnp.dot(later_mask, stats, precision=HIGH, preferred_element_type=jnp.float32)
+    lift = later[:, 0:1] + stats[:, 1:2]
+    parity = lax.broadcasted_iota(jnp.int32, (32, 1), 0) % 2
+    highest = [
+        jnp.max(jnp.where(parity == s, lift, -jnp.inf), axis=0, keepdims=True)
+        for s in range(seqs)
+    ]
+    factor = jnp.exp(lift - jnp.where(parity == 0, highest[0], highest[1]))
+
+    pick = lax.broadcasted_iota(jnp.int32, (heads, dk), 0) == mine
+    ones = jnp.ones((8, span), jnp.bfloat16)
+    aux_row = lax.broadcasted_iota(jnp.int32, (1, 128), 1)
+    tail = jnp.zeros((1, 128), jnp.float32)
+    for s in range(seqs):
+        sums = jnp.zeros((dk, dv), jnp.float32)
+        norms = jnp.zeros((8, dk), jnp.float32)
+        for r in range(4):
+            d = decay[r, s * span : (s + 1) * span]
+            v = vals[r, s * span : (s + 1) * span]
+            f = factor[r * seqs + s : r * seqs + s + 1, 0:1]
+            sums = sums + f * lax.dot_general(
+                d, v, (((0,), (0,)), ((), ())), preferred_element_type=jnp.float32
+            )
+            norms = norms + f * jnp.dot(ones, d, preferred_element_type=jnp.float32)
+        state[s] = sums.astype(jnp.bfloat16)
+        query = jnp.sum(
+            jnp.where(pick, new_query[s].astype(jnp.float32), 0.0), axis=0, keepdims=True
+        )
+        seen = jnp.dot(
+            jnp.broadcast_to(query, (8, dk)),
+            sums,
+            precision=HIGH,
+            preferred_element_type=jnp.float32,
+        )
+        for k in range(dv // 128):
+            aux[s * 4 + k : s * 4 + k + 1] = seen[0:1, k * 128 : (k + 1) * 128]
+        for k in range(dk // 128):
+            row = 8 + s * 2 + k
+            aux[row : row + 1] = norms[0:1, k * 128 : (k + 1) * 128]
+        dot_norm = jnp.sum(query * norms[0:1], axis=1, keepdims=True)
+        tail = jnp.where(aux_row == s, highest[s], tail)
+        tail = jnp.where(aux_row == 2 + s, dot_norm, tail)
+    aux[12:13] = tail
+    aux[13:16] = jnp.zeros((3, 128), jnp.float32)
+
+    def cut_rows(sp):
+        return pl.ds(pl.multiple_of(sp * rows_out, rows_out), rows_out)
+
+    for off in range(1, count):
+        peer = (me + off) % count
+        go(
+            remote(
+                state.at[:, cut_rows(peer)],
+                rmem.at[me],
+                m_send.at[off],
+                m_recv.at[off],
+                peer,
+                core,
+            )
+        )
+        go(remote(aux, raux.at[me], a_send.at[off], a_recv.at[off], peer, core))
+    rmem[me] = state[:, cut_rows(me), :]
+    raux[me] = aux[...]
+
+    def stack(ref):
+        return jnp.concatenate([ref[s].astype(jnp.float32) for s in range(seqs)], axis=0)
+
+    queries = stack(new_query)
+    own = jnp.sum(queries * stack(new_key), axis=1, keepdims=True) * key_scale
+    gate_in, gate_f = new_gates[:, 0:1], log_sigmoid(new_gates[:, 1:2])
+    token_values = stack(new_value)
+
+    for off in range(1, count):
+        src = (me + count - off) % count
+        pltpu.make_async_copy(rmem.at[src], rmem.at[src], m_recv.at[off]).wait()
+        pltpu.make_async_copy(raux.at[src], raux.at[src], a_recv.at[off]).wait()
+
+    read_rows, norm_rows, max_rows, dot_rows = [], [], [], []
+    for s in range(seqs):
+        for h in range(heads):
+            srcs = [
+                a * 8 + (h // 2) * 4 + b * 2 + h % 2 for a in range(2) for b in range(2)
+            ]
+            mem = rmem[srcs[0], s].astype(jnp.float32)
+            both = raux[srcs[0]]
+            for src in srcs[1:]:
+                mem = mem + rmem[src, s].astype(jnp.float32)
+                both = both + raux[src]
+            memory_out[s, h] = mem.astype(jnp.bfloat16)
+            read_rows.append(
+                jnp.concatenate([both[s * 4 + k : s * 4 + k + 1] for k in range(dv // 128)], 1)
+            )
+            norm_rows.append(
+                jnp.concatenate(
+                    [both[8 + s * 2 + k : 9 + s * 2 + k] for k in range(dk // 128)], 1
+                )
+            )
+            max_rows.append(raux[srcs[0], 12:13, s : s + 1])
+            dot_rows.append(both[12:13, 2 + s : 3 + s])
+    query_state = jnp.concatenate(read_rows, axis=0)
+    norm_all = jnp.concatenate(norm_rows, axis=0)
+    top = jnp.concatenate(max_rows, axis=0)
+    query_norm = jnp.concatenate(dot_rows, axis=0)
+    take = (
+        lax.broadcasted_iota(jnp.int32, (dk, rows_out), 0)
+        == me * rows_out + lax.broadcasted_iota(jnp.int32, (dk, rows_out), 1)
+    ).astype(jnp.float32)
+    norm_out[...] = jnp.dot(norm_all, take, precision=HIGH, preferred_element_type=jnp.float32)
+    max_out[...] = top
+    mixed = jnp.maximum(gate_f + top, gate_in)
+    carried = jnp.exp(gate_f + top - mixed)
+    fresh = jnp.exp(gate_in - mixed)
+    numer = carried * query_state + (fresh * own) * token_values
+    denom = carried * query_norm + fresh * own
+    read_out[...] = (numer / jnp.maximum(jnp.abs(denom), 1.0)).astype(jnp.bfloat16)
+    for copy in sent:
+        copy.wait_send()
+
+
+def by_head(
+    prompt,
+    w_key,
+    w_value,
+    w_igate,
+    w_fgate,
+    input_bias,
+    forget_bias,
+    new_query,
+    new_key,
+    new_value,
+    new_gates,
+):
+    count = lax.axis_size("sp")
+    seqs, span, width = prompt.shape
+    depth = w_key.shape[0]
+    heads, dk = new_query.shape[1:]
+    dv = new_value.shape[2]
+    rows = seqs * span
+    w_gate = jnp.concatenate([w_igate, w_fgate], axis=1)
+    gate_bias = jnp.concatenate([input_bias, forget_bias])[None]
+    token_gates = new_gates.reshape(2, seqs * heads).T
+    vmem = pl.BlockSpec(memory_space=pltpu.VMEM)
+    hbm = pl.BlockSpec(memory_space=pl.ANY)
+    dma = pltpu.SemaphoreType.DMA
+    memory, norm, top, read = pl.pallas_call(
+        kernel,
+        out_shape=(
+            jax.ShapeDtypeStruct((seqs, heads, dk // count, dv), jnp.bfloat16),
+            jax.ShapeDtypeStruct((seqs * heads, dk // count), jnp.float32),
+            jax.ShapeDtypeStruct((seqs * heads, 1), jnp.float32),
+            jax.ShapeDtypeStruct((seqs * heads, dv), jnp.bfloat16),
+        ),
+        in_specs=[hbm, hbm, hbm] + [vmem] * 6,
+        out_specs=(vmem, vmem, vmem, vmem),
+        scratch_shapes=[
+            pltpu.VMEM((4, rows, width), jnp.bfloat16),
+            pltpu.VMEM((width, dk), jnp.bfloat16),
+            pltpu.VMEM((width, dv), jnp.bfloat16),
+            pltpu.VMEM((4, rows, dk), jnp.bfloat16),
+            pltpu.VMEM((4, rows, dv), jnp.bfloat16),
+            pltpu.VMEM((4, rows, 128), jnp.float32),
+            pltpu.VMEM((4, 8, 128), jnp.float32),
+            pltpu.VMEM((seqs, dk, dv), jnp.bfloat16),
+            pltpu.VMEM((16, 128), jnp.float32),
+            pltpu.VMEM((count, seqs, dk // count, dv), jnp.bfloat16),
+            pltpu.VMEM((count, 16, 128), jnp.float32),
+            dma((4,)),
+            dma((4, CHUNKS)),
+            dma((4, CHUNKS)),
+            dma((4, CHUNKS)),
+            dma((4, CHUNKS)),
+            dma((16,)),
+            dma((16,)),
+            dma((16,)),
+            dma((16,)),
+            dma((4,)),
+            dma((4,)),
+            dma((count,)),
+            dma((count,)),
+            dma((count,)),
+            dma((count,)),
+        ],
+        compiler_params=pltpu.CompilerParams(
+            collective_id=0, has_side_effects=True, vmem_limit_bytes=60 * 1024 * 1024
+        ),
+    )(prompt, w_key, w_value, w_gate, gate_bias, new_query, new_key, new_value, token_gates)
+    return (
+        memory,
+        norm.reshape(seqs, heads, dk // count),
+        top.reshape(seqs, heads),
+        read.reshape(seqs, heads, dv),
+    )
+
+
+def chosen(*args):
+    prompt, new_query, new_value = args[0], args[7], args[9]
+    heads = new_query.shape[1]
+    count = lax.axis_size("sp")
+    fits = (
+        lax.axis_size("tp") == 2
+        and heads == 4
+        and count == 16
+        and prompt.shape[0] == 2
+        and new_query.shape[2] == 256
+        and new_value.shape[2] == 512
+    )
+    return by_head(*args) if fits else per_device(*args)
 
 
 def entering(value, axis, join, neutral):
@@ -127,7 +636,7 @@
         P(None, None, "tp"),
     )
     return jax.shard_map(
-        per_device,
+        chosen,
         mesh=mesh,
         in_specs=placed,
         out_specs=(

time: 502 us -> 152 us (0.30)
  the two profiles are of different devices: /device:TPU:0 before, /device:TPU:31 now
where the time goes in v1:
time: 152 us; the launch traced here: 151 us
  Pallas kernels  140 us (92%)
  local copies, waits for them, and re-layouts  7.48 us (5%)
  other arithmetic  2.93 us (2%)
    pallas_call x1, Pallas kernels, by_head(): pl.pallas_call(kernel, out_shape=(jax.ShapeDtypeStruct((seqs, heads, dk /...  140 us

profile of v1, /device:TPU:31, one launch (start us, length us, event | category | flops | bytes accessed | tf_op | source)
XLA Modules:
  0.0 151.3 jit_solution(16952835338294838955)
XLA Ops:
  0.6 1.3 maximum_bitcast_fusion.gate_bias
  1.9 1.4 copy.23
  3.2 0.9 pad_maximum_fusion
  4.1 1.3 copy.22.w_gate
  5.5 140.3 %shard_map.138 = (bf16[2,4,16,512]{3,2,1,0:T(8,128)(2,1)}, f32[8,16]{1,0:T(8,128)}, f32[8,1]{1,0:T(8,128)}, bf16[8,512]{1,0:T(8,128)(2,1)}) custom-call(bf16[2,192,4096]{2,1,0:T(8,128)(2,1)} %prompt.1, bf16[256,1024]{1,0:T(8,128)(2,1)} %w_key.1, bf16[256,2048]{1,0:T(8,128)(2,1)} %w_value.1, bf16[4096,16]{1,0:T(8,128)(2,1)} %copy.22.w_gate, ...), custom_call_target="tpu_custom_call" | custom-call | tf_op jit(solution)/shard_map/pallas_call | solution.py:451
  145.7 0.8 reduce
  146.5 0.6 reshape.22
  147.2 1.3 reshape.23
  148.5 1.6 %copy.26 = bf16[2,4,16,512]{3,2,1,0:T(8,128)(2,1)} copy(bf16[2,4,16,512]{3,2,1,0:T(8,128)(2,1)} %get-tuple-element.16) | data formatting | bytes 262144
  150.0 1.3 copy.27

commit v2 on v1

--- a/solution.py
+++ b/solution.py
@@ -6,7 +6,8 @@
 from jax.experimental.pallas import tpu as pltpu
 from jax.sharding import PartitionSpec as P
 
-CHUNKS = 4
+CHUNKS = 8
+PER = CHUNKS // 4
 HIGH = lax.Precision.HIGHEST
 
 
@@ -22,8 +23,10 @@
     prompt,
     w_key,
     w_value,
-    w_gate,
-    gate_bias,
+    w_igate,
+    w_fgate,
+    input_bias,
+    forget_bias,
     new_query,
     new_key,
     new_value,
@@ -35,6 +38,9 @@
     xb,
     wk,
     wv,
+    w_gate,
+    key_acc,
+    value_acc,
     decay,
     vals,
     weight,
@@ -67,7 +73,7 @@
     heads = new_query.shape[1]
     dk = new_query.shape[2]
     dv = new_value.shape[2]
-    total_heads = gate_bias.shape[1] // 2
+    total_heads = input_bias.shape[1]
     key_scale = dk ** (-0.5)
     cut = width // CHUNKS
     rows_out = dk // count
@@ -181,7 +187,8 @@
         part = x_part(slot, other_rows, k)
         pltpu.make_async_copy(part, part, d_recv.at[slot, k]).wait()
 
-    x_send_own(2, 0, to_z)
+    for k in range(PER):
+        x_send_own(2, k, to_z)
     for k in range(CHUNKS):
         x_send_own(1, k, to_x)
     own_k.wait()
@@ -192,12 +199,17 @@
         w_wait(r)
         w_relay(r, (1, 0), 4 + r)
         w_relay(r, (0, 1), 8 + r)
-        x_send_own(2, r, to_z)
+        for k in range(PER):
+            x_send_own(2, r * PER + k, to_z)
     for c in own_x:
         c.wait()
 
     lane = lax.broadcasted_iota(jnp.int32, (seqs * span, 2 * total_heads), 1)
     head = core * heads + mine
+    w_gate[...] = jnp.concatenate([w_igate[...], w_fgate[...]], axis=0)
+    head_lane = lax.broadcasted_iota(jnp.int32, (1, total_heads), 1) == head
+    bias_in = jnp.sum(jnp.where(head_lane, input_bias[...], 0.0), axis=1, keepdims=True)
+    bias_f = jnp.sum(jnp.where(head_lane, forget_bias[...], 0.0), axis=1, keepdims=True)
     at_t = lax.broadcasted_iota(jnp.int32, (span, span), 0)
     at_u = lax.broadcasted_iota(jnp.int32, (span, span), 1)
     after = (at_u > at_t).astype(jnp.float32)
@@ -205,9 +217,14 @@
     stat_lane = lax.broadcasted_iota(jnp.int32, (8, 128), 1)
 
     def gates(r, table):
-        both = jnp.dot(xb[r], w_gate[...], preferred_element_type=jnp.float32) + gate_bias[...]
-        gate_in = jnp.sum(jnp.where(lane == head, both, 0.0), axis=1, keepdims=True)
-        gate_f = jnp.sum(
+        both = lax.dot_general(
+            xb[r],
+            w_gate[...],
+            (((1,), (1,)), ((), ())),
+            preferred_element_type=jnp.float32,
+        )
+        gate_in = bias_in + jnp.sum(jnp.where(lane == head, both, 0.0), axis=1, keepdims=True)
+        gate_f = bias_f + jnp.sum(
             jnp.where(lane == total_heads + head, both, 0.0), axis=1, keepdims=True
         )
         forget = log_sigmoid(gate_f)
@@ -226,63 +243,91 @@
             table = jnp.where(hit & (stat_lane == 1), top, table)
         return table
 
+    def project(r, slots, first):
+        def step(i, carry):
+            keys = values = None
+            for off in range(2):
+                rows = slots(2 * i + off)
+                tokens = xb[r, :, rows]
+                k_part = jnp.dot(tokens, wk[rows], preferred_element_type=jnp.float32)
+                v_part = jnp.dot(tokens, wv[rows], preferred_element_type=jnp.float32)
+                keys = k_part if keys is None else keys + k_part
+                values = v_part if values is None else values + v_part
+            key_acc[r] += keys
+            value_acc[r] += values
+            return carry
+
+        if first:
+            key_acc[r] = jnp.zeros((seqs * span, dk), jnp.float32)
+            value_acc[r] = jnp.zeros((seqs * span, dv), jnp.float32)
+        return step
+
+    def source_rows(q):
+        def rows(r):
+            dh, dy = clique[q]
+            dz, dx = r // 2, r % 2
+            src = place(dh, dy, dz, dx)
+            return pl.ds(pl.multiple_of(src * depth, depth), depth)
+
+        return rows
+
+    def group(r, q, first=False):
+        lax.fori_loop(0, 2, project(r, source_rows(q), first), 0)
+
+    def finish(r):
+        keys = key_acc[r].astype(jnp.bfloat16).astype(jnp.float32)
+        decay[r] = (weight[r, :, 0:1] * keys).astype(jnp.bfloat16)
+        vals[r] = value_acc[r].astype(jnp.bfloat16)
+
     table = gates(0, jnp.zeros((8, 128), jnp.float32))
-    for k in range(CHUNKS):
+    group(0, 0, True)
+    for k in range(4):
         w_wait(8 + k)
         w_relay(8 + k, (0, 1), 12 + k)
-        x_wait(2, k)
-        go(
-            remote(
-                x_part(2, my_rows, k),
-                x_part(3, my_rows, k),
-                x_send.at[3, k],
-                x_recv.at[3, k],
-                to_x,
-                core,
+        for c in range(k * PER, (k + 1) * PER):
+            x_wait(2, c)
+            go(
+                remote(
+                    x_part(2, my_rows, c),
+                    x_part(3, my_rows, c),
+                    x_send.at[3, c],
+                    x_recv.at[3, c],
+                    to_x,
+                    core,
+                )
             )
-        )
-        x_across(2, k)
-        x_wait(1, k)
-        x_across(1, k)
-    for k in range(CHUNKS):
-        d_wait(1, k)
-        d_wait(2, k)
+            x_across(2, c)
+            x_wait(1, c)
+            x_across(1, c)
+    group(0, 2)
+    for slot in range(4, 8):
+        w_wait(slot)
+    group(0, 1)
+    for c in range(CHUNKS):
+        d_wait(1, c)
     table = gates(1, table)
+    for q in range(3):
+        group(1, q, q == 0)
+    for c in range(CHUNKS // 2):
+        x_wait(3, c)
+        x_across(3, c)
+    for c in range(CHUNKS):
+        d_wait(2, c)
     table = gates(2, table)
-    for k in range(CHUNKS):
-        x_wait(3, k)
-        x_across(3, k)
-    for k in range(CHUNKS):
-        d_wait(3, k)
+    for q in range(3):
+        group(2, q, q == 0)
+    for c in range(CHUNKS // 2, CHUNKS):
+        x_wait(3, c)
+        x_across(3, c)
+    for slot in range(12, 16):
+        w_wait(slot)
+    for c in range(CHUNKS):
+        d_wait(3, c)
     table = gates(3, table)
     stat[0] = table
-    for slot in (4, 5, 6, 7, 12, 13, 14, 15):
-        w_wait(slot)
-
-    def project(r, carry):
-        def step(k, acc):
-            at = pl.ds(pl.multiple_of(k * cut, cut), cut)
-            rows = xb[r, :, at]
-            return (
-                acc[0] + jnp.dot(rows, wk[at], preferred_element_type=jnp.float32),
-                acc[1] + jnp.dot(rows, wv[at], preferred_element_type=jnp.float32),
-            )
-
-        keys, values = lax.fori_loop(
-            0,
-            CHUNKS,
-            step,
-            (
-                jnp.zeros((seqs * span, dk), jnp.float32),
-                jnp.zeros((seqs * span, dv), jnp.float32),
-            ),
-        )
-        keys = keys.astype(jnp.bfloat16).astype(jnp.float32)
-        decay[r] = (weight[r, :, 0:1] * keys).astype(jnp.bfloat16)
-        vals[r] = values.astype(jnp.bfloat16)
-        return carry
-
-    project(0, 0)
+    for r in range(3):
+        group(r, 3)
+        finish(r)
     for q in (1, 2, 3):
         dh, dy = clique[q]
         go(
@@ -290,7 +335,9 @@
                 stat.at[0], stat.at[q], s_send.at[q], s_recv.at[q], place(dh, dy, 0, 0), core
             )
         )
-    lax.fori_loop(1, 4, project, 0)
+    for q in range(4):
+        group(3, q, q == 0)
+    finish(3)
     for q in (1, 2, 3):
         pltpu.make_async_copy(stat.at[q], stat.at[q], s_recv.at[q]).wait()
 
@@ -317,6 +364,10 @@
     ones = jnp.ones((8, span), jnp.bfloat16)
     aux_row = lax.broadcasted_iota(jnp.int32, (1, 128), 1)
     tail = jnp.zeros((1, 128), jnp.float32)
+
+    def cut_rows(sp):
+        return pl.ds(pl.multiple_of(sp * rows_out, rows_out), rows_out)
+
     for s in range(seqs):
         sums = jnp.zeros((dk, dv), jnp.float32)
         norms = jnp.zeros((8, dk), jnp.float32)
@@ -346,24 +397,22 @@
         dot_norm = jnp.sum(query * norms[0:1], axis=1, keepdims=True)
         tail = jnp.where(aux_row == s, highest[s], tail)
         tail = jnp.where(aux_row == 2 + s, dot_norm, tail)
+        for off in range(1, count):
+            peer = (me + off) % count
+            go(
+                remote(
+                    state.at[s, cut_rows(peer)],
+                    rmem.at[me, s],
+                    m_send.at[s, off],
+                    m_recv.at[s, off],
+                    peer,
+                    core,
+                )
+            )
     aux[12:13] = tail
     aux[13:16] = jnp.zeros((3, 128), jnp.float32)
-
-    def cut_rows(sp):
-        return pl.ds(pl.multiple_of(sp * rows_out, rows_out), rows_out)
-
     for off in range(1, count):
         peer = (me + off) % count
-        go(
-            remote(
-                state.at[:, cut_rows(peer)],
-                rmem.at[me],
-                m_send.at[off],
-                m_recv.at[off],
-                peer,
-                core,
-            )
-        )
         go(remote(aux, raux.at[me], a_send.at[off], a_recv.at[off], peer, core))
     rmem[me] = state[:, cut_rows(me), :]
     raux[me] = aux[...]
@@ -373,12 +422,25 @@
 
     queries = stack(new_query)
     own = jnp.sum(queries * stack(new_key), axis=1, keepdims=True) * key_scale
-    gate_in, gate_f = new_gates[:, 0:1], log_sigmoid(new_gates[:, 1:2])
+    own_head = (
+        lax.broadcasted_iota(jnp.int32, (seqs * heads, heads), 0) % heads
+        == lax.broadcasted_iota(jnp.int32, (seqs * heads, heads), 1)
+    )
+
+    def upright(block):
+        wide = jnp.concatenate(
+            [jnp.broadcast_to(block[s : s + 1], (heads, heads)) for s in range(seqs)], axis=0
+        )
+        return jnp.sum(jnp.where(own_head, wide, 0.0), axis=1, keepdims=True)
+
+    gate_in, gate_f = upright(new_gates[0]), log_sigmoid(upright(new_gates[1]))
     token_values = stack(new_value)
 
     for off in range(1, count):
         src = (me + count - off) % count
-        pltpu.make_async_copy(rmem.at[src], rmem.at[src], m_recv.at[off]).wait()
+        for s in range(seqs):
+            part = rmem.at[src, s]
+            pltpu.make_async_copy(part, part, m_recv.at[s, off]).wait()
         pltpu.make_async_copy(raux.at[src], raux.at[src], a_recv.at[off]).wait()
 
     read_rows, norm_rows, max_rows, dot_rows = [], [], [], []
@@ -423,6 +485,21 @@
         copy.wait_send()
 
 
+def hand_on(memory, norm, top, read, memory_out, norm_out, max_out, read_out):
+    seqs, heads = max_out.shape
+    memory_out[...] = memory[...]
+    at = lax.broadcasted_iota(jnp.int32, (seqs * heads, heads), 0)
+    to = lax.broadcasted_iota(jnp.int32, (seqs * heads, heads), 1)
+    wide = read[...].astype(jnp.float32)
+    for s in range(seqs):
+        rows = slice(s * heads, (s + 1) * heads)
+        norm_out[s] = norm[rows]
+        read_out[s] = wide[rows].astype(jnp.bfloat16)
+        max_out[s : s + 1] = jnp.sum(
+            jnp.where(at == s * heads + to, top[...], 0.0), axis=0, keepdims=True
+        )
+
+
 def by_head(
     prompt,
     w_key,
@@ -442,9 +519,6 @@
     heads, dk = new_query.shape[1:]
     dv = new_value.shape[2]
     rows = seqs * span
-    w_gate = jnp.concatenate([w_igate, w_fgate], axis=1)
-    gate_bias = jnp.concatenate([input_bias, forget_bias])[None]
-    token_gates = new_gates.reshape(2, seqs * heads).T
     vmem = pl.BlockSpec(memory_space=pltpu.VMEM)
     hbm = pl.BlockSpec(memory_space=pl.ANY)
     dma = pltpu.SemaphoreType.DMA
@@ -456,12 +530,15 @@
             jax.ShapeDtypeStruct((seqs * heads, 1), jnp.float32),
             jax.ShapeDtypeStruct((seqs * heads, dv), jnp.bfloat16),
         ),
-        in_specs=[hbm, hbm, hbm] + [vmem] * 6,
+        in_specs=[hbm, hbm, hbm] + [vmem] * 8,
         out_specs=(vmem, vmem, vmem, vmem),
         scratch_shapes=[
             pltpu.VMEM((4, rows, width), jnp.bfloat16),
             pltpu.VMEM((width, dk), jnp.bfloat16),
             pltpu.VMEM((width, dv), jnp.bfloat16),
+            pltpu.VMEM((2 * w_igate.shape[1], width), jnp.bfloat16),
+            pltpu.VMEM((4, rows, dk), jnp.float32),
+            pltpu.VMEM((4, rows, dv), jnp.float32),
             pltpu.VMEM((4, rows, dk), jnp.bfloat16),
             pltpu.VMEM((4, rows, dv), jnp.bfloat16),
             pltpu.VMEM((4, rows, 128), jnp.float32),
@@ -481,21 +558,38 @@
             dma((16,)),
             dma((4,)),
             dma((4,)),
-            dma((count,)),
-            dma((count,)),
+            dma((seqs, count)),
+            dma((seqs, count)),
             dma((count,)),
             dma((count,)),
         ],
         compiler_params=pltpu.CompilerParams(
             collective_id=0, has_side_effects=True, vmem_limit_bytes=60 * 1024 * 1024
         ),
-    )(prompt, w_key, w_value, w_gate, gate_bias, new_query, new_key, new_value, token_gates)
-    return (
-        memory,
-        norm.reshape(seqs, heads, dk // count),
-        top.reshape(seqs, heads),
-        read.reshape(seqs, heads, dv),
-    )
+    )(
+        prompt,
+        w_key,
+        w_value,
+        w_igate.T,
+        w_fgate.T,
+        input_bias[None],
+        forget_bias[None],
+        new_query,
+        new_key,
+        new_value,
+        new_gates,
+    )
+    return pl.pallas_call(
+        hand_on,
+        out_shape=(
+            jax.ShapeDtypeStruct((seqs, heads, dk // count, dv), jnp.bfloat16),
+            jax.ShapeDtypeStruct((seqs, heads, dk // count), jnp.float32),
+            jax.ShapeDtypeStruct((seqs, heads), jnp.float32),
+            jax.ShapeDtypeStruct((seqs, heads, dv), jnp.bfloat16),
+        ),
+        in_specs=[vmem] * 4,
+        out_specs=(vmem,) * 4,
+    )(memory, norm, top, read)
 
 
 def chosen(*args):

time: 152 us -> 140 us (0.921)
  the two profiles are of different devices: /device:TPU:31 before, /device:TPU:0 now
where the time goes in v2:
time: 140 us; the launch traced here: 139 us
  Pallas kernels  139 us (99%)
    pallas_call x1, Pallas kernels, by_head(): pl.pallas_call(kernel, out_shape=(jax.ShapeDtypeStruct((seqs, heads, dk /...  137 us

profile of v2, /device:TPU:0, one launch (start us, length us, event | category | flops | bytes accessed | tf_op | source)
XLA Modules:
  0.0 139.3 jit_solution(16659267011988987917)
XLA Ops:
  0.6 137.1 %shard_map.138 = (bf16[2,4,16,512]{3,2,1,0:T(8,128)(2,1)}, f32[8,16]{1,0:T(8,128)}, f32[8,1]{1,0:T(8,128)}, bf16[8,512]{1,0:T(8,128)(2,1)}) custom-call(bf16[2,192,4096]{2,1,0:T(8,128)(2,1)} %prompt.1, bf16[256,1024]{1,0:T(8,128)(2,1)} %w_key.1, bf16[256,2048]{1,0:T(8,128)(2,1)} %w_value.1, bf16[8,4096]{1,0:T(8,128)(2,1)} %bitcast.4, ...), custom_call_target="tpu_custom_call" | custom-call | tf_op jit(solution)/shard_map/pallas_call | solution.py:525
  137.8 1.6 %shard_map.139 = (bf16[2,4,16,512]{3,2,1,0:T(8,128)(2,1)}, f32[2,4,16]{2,1,0:T(4,128)}, f32[2,4]{1,0:T(2,128)}, bf16[2,4,512]{2,1,0:T(4,128)(2,1)}) custom-call(bf16[2,4,16,512]{3,2,1,0:T(8,128)(2,1)} %get-tuple-element.8.memory, f32[8,16]{1,0:T(8,128)} %get-tuple-element.9.norm, f32[8,1]{1,0:T(8,128)} %get-tuple-element.10.top, ...), custom_call_target="tpu_custom_call" | custom-call | tf_op jit(solution)/shard_map/pallas_call | solution.py:582

commit v3 on v2

--- a/solution.py
+++ b/solution.py
@@ -282,8 +282,6 @@
     table = gates(0, jnp.zeros((8, 128), jnp.float32))
     group(0, 0, True)
     for k in range(4):
-        w_wait(8 + k)
-        w_relay(8 + k, (0, 1), 12 + k)
         for c in range(k * PER, (k + 1) * PER):
             x_wait(2, c)
             go(
@@ -297,17 +295,23 @@
                 )
             )
             x_across(2, c)
-            x_wait(1, c)
-            x_across(1, c)
+        w_wait(8 + k)
+        w_relay(8 + k, (0, 1), 12 + k)
+        if k == 1:
+            for c in range(CHUNKS):
+                x_wait(1, c)
+                x_across(1, c)
+            for slot in range(4, 8):
+                w_wait(slot)
+            group(0, 1)
+        if k == 2:
+            for c in range(CHUNKS):
+                d_wait(1, c)
+            table = gates(1, table)
+            group(1, 0, True)
+            group(1, 1)
     group(0, 2)
-    for slot in range(4, 8):
-        w_wait(slot)
-    group(0, 1)
-    for c in range(CHUNKS):
-        d_wait(1, c)
-    table = gates(1, table)
-    for q in range(3):
-        group(1, q, q == 0)
+    group(1, 2)
     for c in range(CHUNKS // 2):
         x_wait(3, c)
         x_across(3, c)

time: 140 us -> 135 us (0.964)
  Pallas kernels: 139 us -> 134 us
    pallas_call x1, Pallas kernels: 137 us -> 132 us  [by_head(): pl.pallas_call(kernel, out_shape=(jax.ShapeDtypeStruct((seqs, heads, dk /...]
where the time goes in v3:
time: 135 us
  Pallas kernels  134 us (99%)
    pallas_call x1, Pallas kernels, by_head(): pl.pallas_call(kernel, out_shape=(jax.ShapeDtypeStruct((seqs, heads, dk /...  132 us

profile of v3, /device:TPU:0, one launch (start us, length us, event | category | flops | bytes accessed | tf_op | source)
XLA Modules:
  0.0 134.7 jit_solution(2885082517521094694)
XLA Ops:
  0.6 132.4 %shard_map.138 = (bf16[2,4,16,512]{3,2,1,0:T(8,128)(2,1)}, f32[8,16]{1,0:T(8,128)}, f32[8,1]{1,0:T(8,128)}, bf16[8,512]{1,0:T(8,128)(2,1)}) custom-call(bf16[2,192,4096]{2,1,0:T(8,128)(2,1)} %prompt.1, bf16[256,1024]{1,0:T(8,128)(2,1)} %w_key.1, bf16[256,2048]{1,0:T(8,128)(2,1)} %w_value.1, bf16[8,4096]{1,0:T(8,128)(2,1)} %bitcast.4, ...), custom_call_target="tpu_custom_call" | custom-call | tf_op jit(solution)/shard_map/pallas_call | solution.py:529
  133.1 1.6 %shard_map.139 = (bf16[2,4,16,512]{3,2,1,0:T(8,128)(2,1)}, f32[2,4,16]{2,1,0:T(4,128)}, f32[2,4]{1,0:T(2,128)}, bf16[2,4,512]{2,1,0:T(4,128)(2,1)}) custom-call(bf16[2,4,16,512]{3,2,1,0:T(8,128)(2,1)} %get-tuple-element.8.memory, f32[8,16]{1,0:T(8,128)} %get-tuple-element.9.norm, f32[8,1]{1,0:T(8,128)} %get-tuple-element.10.top, ...), custom_call_target="tpu_custom_call" | custom-call | tf_op jit(solution)/shard_map/pallas_call | solution.py:586

commit v4 on v3

--- a/solution.py
+++ b/solution.py
@@ -47,6 +47,10 @@
     stat,
     state,
     aux,
+    yin,
+    yaux,
+    total_state,
+    total_aux,
     rmem,
     raux,
     local_sem,
@@ -60,6 +64,8 @@
     wv_recv,
     s_send,
     s_recv,
+    y_send,
+    y_recv,
     m_send,
     m_recv,
     a_send,
@@ -369,8 +375,12 @@
     aux_row = lax.broadcasted_iota(jnp.int32, (1, 128), 1)
     tail = jnp.zeros((1, 128), jnp.float32)
 
-    def cut_rows(sp):
-        return pl.ds(pl.multiple_of(sp * rows_out, rows_out), rows_out)
+    to_y = place(0, 1, 0, 0)
+    half = count // 2
+    spot8 = (zh * 2 + zl) * 2 + x
+
+    def cut_rows(spot):
+        return pl.ds(pl.multiple_of(spot * rows_out, rows_out), rows_out)
 
     for s in range(seqs):
         sums = jnp.zeros((dk, dv), jnp.float32)
@@ -383,7 +393,10 @@
                 d, v, (((0,), (0,)), ((), ())), preferred_element_type=jnp.float32
             )
             norms = norms + f * jnp.dot(ones, d, preferred_element_type=jnp.float32)
-        state[s] = sums.astype(jnp.bfloat16)
+        for block in range(count // 2):
+            rows = sums[block * 2 * rows_out : (block + 1) * 2 * rows_out]
+            low = (block // 2) * 2 * rows_out
+            state[s, block % 2, low : low + 2 * rows_out] = rows.astype(jnp.bfloat16)
         query = jnp.sum(
             jnp.where(pick, new_query[s].astype(jnp.float32), 0.0), axis=0, keepdims=True
         )
@@ -401,25 +414,51 @@
         dot_norm = jnp.sum(query * norms[0:1], axis=1, keepdims=True)
         tail = jnp.where(aux_row == s, highest[s], tail)
         tail = jnp.where(aux_row == 2 + s, dot_norm, tail)
-        for off in range(1, count):
-            peer = (me + off) % count
+        go(
+            remote(state.at[s, 1 - y], yin.at[s], y_send.at[s], y_recv.at[s], to_y, core)
+        )
+    aux[12:13] = tail
+    aux[13:16] = jnp.zeros((3, 128), jnp.float32)
+    go(remote(aux, yaux, y_send.at[2], y_recv.at[2], to_y, core))
+
+    def of_spot(spot):
+        return (spot // 2) * 4 + y * 2 + spot % 2
+
+    for s in range(seqs):
+        pltpu.make_async_copy(yin.at[s], yin.at[s], y_recv.at[s]).wait()
+        total_state[s] = (
+            state[s, y].astype(jnp.float32) + yin[s].astype(jnp.float32)
+        ).astype(jnp.bfloat16)
+        for off in range(1, half):
+            spot = (spot8 + off) % half
             go(
                 remote(
-                    state.at[s, cut_rows(peer)],
-                    rmem.at[me, s],
+                    total_state.at[s, cut_rows(spot)],
+                    rmem.at[spot8, s],
                     m_send.at[s, off],
                     m_recv.at[s, off],
-                    peer,
+                    of_spot(spot),
                     core,
                 )
             )
-    aux[12:13] = tail
-    aux[13:16] = jnp.zeros((3, 128), jnp.float32)
-    for off in range(1, count):
-        peer = (me + off) % count
-        go(remote(aux, raux.at[me], a_send.at[off], a_recv.at[off], peer, core))
-    rmem[me] = state[:, cut_rows(me), :]
-    raux[me] = aux[...]
+        rmem[spot8, s] = total_state[s, cut_rows(spot8), :]
+    pltpu.make_async_copy(yaux, yaux, y_recv.at[2]).wait()
+    keep = (lax.broadcasted_iota(jnp.int32, (16, 128), 0) == 12) & (
+        lax.broadcasted_iota(jnp.int32, (16, 128), 1) < seqs
+    )
+    total_aux[...] = jnp.where(keep, aux[...], aux[...] + yaux[...])
+    for off in range(1, half):
+        go(
+            remote(
+                total_aux,
+                raux.at[spot8],
+                a_send.at[off],
+                a_recv.at[off],
+                of_spot((spot8 + off) % half),
+                core,
+            )
+        )
+    raux[spot8] = total_aux[...]
 
     def stack(ref):
         return jnp.concatenate([ref[s].astype(jnp.float32) for s in range(seqs)], axis=0)
@@ -440,8 +479,8 @@
     gate_in, gate_f = upright(new_gates[0]), log_sigmoid(upright(new_gates[1]))
     token_values = stack(new_value)
 
-    for off in range(1, count):
-        src = (me + count - off) % count
+    for off in range(1, half):
+        src = (spot8 + half - off) % half
         for s in range(seqs):
             part = rmem.at[src, s]
             pltpu.make_async_copy(part, part, m_recv.at[s, off]).wait()
@@ -450,9 +489,7 @@
     read_rows, norm_rows, max_rows, dot_rows = [], [], [], []
     for s in range(seqs):
         for h in range(heads):
-            srcs = [
-                a * 8 + (h // 2) * 4 + b * 2 + h % 2 for a in range(2) for b in range(2)
-            ]
+            srcs = [(a * 2 + h // 2) * 2 + h % 2 for a in range(2)]
             mem = rmem[srcs[0], s].astype(jnp.float32)
             both = raux[srcs[0]]
             for src in srcs[1:]:
@@ -547,10 +584,14 @@
             pltpu.VMEM((4, rows, dv), jnp.bfloat16),
             pltpu.VMEM((4, rows, 128), jnp.float32),
             pltpu.VMEM((4, 8, 128), jnp.float32),
-            pltpu.VMEM((seqs, dk, dv), jnp.bfloat16),
+            pltpu.VMEM((seqs, 2, dk // 2, dv), jnp.bfloat16),
             pltpu.VMEM((16, 128), jnp.float32),
-            pltpu.VMEM((count, seqs, dk // count, dv), jnp.bfloat16),
-            pltpu.VMEM((count, 16, 128), jnp.float32),
+            pltpu.VMEM((seqs, dk // 2, dv), jnp.bfloat16),
+            pltpu.VMEM((16, 128), jnp.float32),
+            pltpu.VMEM((seqs, dk // 2, dv), jnp.bfloat16),
+            pltpu.VMEM((16, 128), jnp.float32),
+            pltpu.VMEM((count // 2, seqs, dk // count, dv), jnp.bfloat16),
+            pltpu.VMEM((count // 2, 16, 128), jnp.float32),
             dma((4,)),
             dma((4, CHUNKS)),
             dma((4, CHUNKS)),
@@ -562,6 +603,8 @@
             dma((16,)),
             dma((4,)),
             dma((4,)),
+            dma((3,)),
+            dma((3,)),
             dma((seqs, count)),
             dma((seqs, count)),
             dma((count,)),

time: 135 us -> 133 us (0.985)
  Pallas kernels: 134 us -> 132 us
    pallas_call x1, Pallas kernels: 132 us -> 130 us  [by_head(): pl.pallas_call(kernel, out_shape=(jax.ShapeDtypeStruct((seqs, heads, dk /...]
where the time goes in v4:
time: 133 us
  Pallas kernels  132 us (99%)
    pallas_call x1, Pallas kernels, by_head(): pl.pallas_call(kernel, out_shape=(jax.ShapeDtypeStruct((seqs, heads, dk /...  130 us

profile of v4, /device:TPU:0, one launch (start us, length us, event | category | flops | bytes accessed | tf_op | source)
XLA Modules:
  0.0 132.6 jit_solution(6391307283061843121)
XLA Ops:
  0.6 130.4 %shard_map.138 = (bf16[2,4,16,512]{3,2,1,0:T(8,128)(2,1)}, f32[8,16]{1,0:T(8,128)}, f32[8,1]{1,0:T(8,128)}, bf16[8,512]{1,0:T(8,128)(2,1)}) custom-call(bf16[2,192,4096]{2,1,0:T(8,128)(2,1)} %prompt.1, bf16[256,1024]{1,0:T(8,128)(2,1)} %w_key.1, bf16[256,2048]{1,0:T(8,128)(2,1)} %w_value.1, bf16[8,4096]{1,0:T(8,128)(2,1)} %bitcast.4, ...), custom_call_target="tpu_custom_call" | custom-call | tf_op jit(solution)/shard_map/pallas_call | solution.py:566
  131.1 1.6 %shard_map.139 = (bf16[2,4,16,512]{3,2,1,0:T(8,128)(2,1)}, f32[2,4,16]{2,1,0:T(4,128)}, f32[2,4]{1,0:T(2,128)}, bf16[2,4,512]{2,1,0:T(4,128)(2,1)}) custom-call(bf16[2,4,16,512]{3,2,1,0:T(8,128)(2,1)} %get-tuple-element.8.memory, f32[8,16]{1,0:T(8,128)} %get-tuple-element.9.norm, f32[8,1]{1,0:T(8,128)} %get-tuple-element.10.top, ...), custom_call_target="tpu_custom_call" | custom-call | tf_op jit(solution)/shard_map/pallas_call | solution.py:629
